TPU v7x, 32 devices: a whole 2x2x4 slice. The times are simulated.
32 devices in a mesh: sp: 8 (over z, y), tp: 4 (over x, core).
Axes of the slice: x: 2, y: 2, z: 4, core: 2. Of those that a mesh axis runs over, the one named last changes fastest.
Arguments:
- query_a: bfloat16 [1536, 2048], P('sp', 'tp'), may hold values from -7.5 to 7.5
- key_a: bfloat16 [1536, 1024], P('sp', 'tp'), may hold values from -7.5 to 7.5
- value_a: bfloat16 [1536, 1024], P('sp', 'tp'), may hold values from -6 to 6
- query_b: bfloat16 [1536, 2048], P('sp', 'tp'), may hold values from -7.5 to 7.5
- key_b: bfloat16 [1536, 512], P('sp', 'tp'), may hold values from -7.5 to 7.5
- value_b: bfloat16 [1536, 512], P('sp', 'tp'), may hold values from -6 to 6
- gain_a: float32 [2, 128], replicated, may hold values from 1 to 6.5
- gain_b: float32 [2, 64], replicated, may hold values from 1 to 8.5
- out_a: bfloat16 [2048, 4096], P('tp'), may hold values from -0.5 to 0.5
- out_b: bfloat16 [2048, 4096], P('tp'), may hold values from -0.5 to 0.5
- residual: bfloat16 [1536, 4096], P('sp'), may hold values from -6 to 6
- norm_gain: float32 [4096], replicated, may hold values from 0.1 to 1.9
- gate_weight: bfloat16 [4096, 6144], P('sp', 'tp'), may hold values from -0.09375 to 0.09375
- up_weight: bfloat16 [4096, 6144], P('sp', 'tp'), may hold values from -0.09375 to 0.09375
- down_weight: bfloat16 [6144, 4096], P('tp', 'sp'), may hold values from -0.3125 to 0.3125
Outputs:
- output: bfloat16 [1536, 4096], P(('sp', 'tp'))
All inputs are finite; a program needn't handle non-finite values.
Results may differ from a plain program's by a relative error of at most 0.017.
The roundings to bfloat16 on the way count: a program that leaves them out, or rounds other values in their place, can miss the bound.
Values may be sent and summed in bfloat16 or wider, within the bound.
A program may use at most 128 MiB of HBM per device.

v0:
```python
import jax
import jax.numpy as jnp
from jax import lax
from jax.sharding import PartitionSpec as P

HEAD_A = 128
HEAD_B = 64
GRID_W = 64


epsilon = 1e-06
theta_base = 10000.0


def rotate(inputs, num_heads, head_size, first_pos, gain):
    tok_rows = inputs.shape[0]
    vectors = inputs.astype(jnp.float32).reshape(tok_rows, num_heads, head_size)
    vectors = (
        vectors * lax.rsqrt(jnp.mean(vectors * vectors, axis=-1, keepdims=True) + epsilon) * gain
    )
    position = first_pos + jnp.arange(tok_rows, dtype=jnp.int32)
    grid_row = (position // GRID_W).astype(jnp.float32)
    grid_col = (position % GRID_W).astype(jnp.float32)
    quarter = head_size // 4
    inv_freq = theta_base ** (-4.0 * jnp.arange(quarter, dtype=jnp.float32) / head_size)
    angle_row = grid_row[:, None] * inv_freq[None, :]
    angle_col = grid_col[:, None] * inv_freq[None, :]
    angles = jnp.concatenate([angle_row, angle_row, angle_col, angle_col], axis=-1)
    quarters = vectors.reshape(tok_rows, num_heads, 4, quarter)
    rotated = jnp.stack(
        [-quarters[:, :, 1], quarters[:, :, 0], -quarters[:, :, 3], quarters[:, :, 2]], axis=2
    )
    rotated = rotated.reshape(tok_rows, num_heads, head_size)
    result = vectors * jnp.cos(angles)[:, None, :] + rotated * jnp.sin(angles)[:, None, :]
    return result.reshape(tok_rows, num_heads * head_size).astype(jnp.bfloat16)


def start_state(kv_heads, groups, tok_rows, head_size):
    return (
        jnp.full((kv_heads, groups, tok_rows), -1e30, jnp.float32),
        jnp.zeros((kv_heads, groups, tok_rows), jnp.float32),
        jnp.zeros((kv_heads, groups, tok_rows, head_size), jnp.float32),
    )


def attend(state, queries, key_rows, values, head_size):
    run_max, run_sum, run_acc = state
    kv_heads = key_rows.shape[1] // head_size
    groups = run_max.shape[1]
    q_heads = queries.reshape(queries.shape[0], kv_heads, groups, head_size)
    k_heads = key_rows.reshape(key_rows.shape[0], kv_heads, head_size)
    v_heads = values.reshape(values.shape[0], kv_heads, head_size)
    scores = jnp.einsum(
        "tkgd,pkd->kgtp", q_heads, k_heads, preferred_element_type=jnp.float32
    ) * head_size ** (-0.5)
    new_max = jnp.maximum(run_max, jnp.max(scores, axis=-1))
    exp_scores = jnp.exp(scores - new_max[..., None])
    new_sum = jnp.sum(exp_scores, axis=-1)
    new_acc = jnp.einsum(
        "kgtp,pkd->kgtd",
        exp_scores.astype(jnp.bfloat16),
        v_heads,
        preferred_element_type=jnp.float32,
    )
    return (new_max, new_sum, new_acc)


def finish(state, num_cols):
    blended = state[2] / state[1][..., None]
    return blended.transpose(2, 0, 1, 3).reshape(blended.shape[2], num_cols).astype(jnp.bfloat16)


def normalize(mixed_rows, gain):
    scale = lax.rsqrt(jnp.mean(mixed_rows * mixed_rows, axis=-1, keepdims=True) + epsilon)
    return (mixed_rows * scale * gain).astype(jnp.bfloat16)


def on_device(
    query_a,
    key_a,
    value_a,
    query_b,
    key_b,
    value_b,
    gain_a,
    gain_b,
    out_a,
    out_b,
    residual,
    norm_gain,
    gate_weight,
    up_weight,
    down_weight,
):
    tok_rows = query_a.shape[0]
    first_pos = lax.axis_index("sp") * tok_rows
    heads_a = query_a.shape[1] // HEAD_A
    heads_b = query_b.shape[1] // HEAD_B
    kv_heads_a = key_a.shape[1] // HEAD_A
    kv_heads_b = key_b.shape[1] // HEAD_B
    kv_width_b = kv_heads_b * HEAD_B
    turned_qa = rotate(query_a, heads_a, HEAD_A, first_pos, gain_a[0])
    turned_ka = rotate(key_a, kv_heads_a, HEAD_A, first_pos, gain_a[1])
    turned_qb = rotate(query_b, heads_b, HEAD_B, first_pos, gain_b[0])
    turned_kb = rotate(key_b, kv_heads_b, HEAD_B, first_pos, gain_b[1])
    pair_b = jnp.concatenate([turned_kb, value_b], axis=1)
    initial = (
        start_state(kv_heads_a, heads_a // kv_heads_a, tok_rows, HEAD_A),
        start_state(kv_heads_b, heads_b // kv_heads_b, tok_rows, HEAD_B),
    )
    pieces = (
        lax.all_gather(turned_ka, "sp", axis=0, tiled=True),
        lax.all_gather(value_a, "sp", axis=0, tiled=True),
        lax.all_gather(pair_b, "sp", axis=0, tiled=True),
    )
    state_a = attend(initial[0], turned_qa, pieces[0], pieces[1], HEAD_A)
    state_b = attend(
        initial[1], turned_qb, pieces[2][:, :kv_width_b], pieces[2][:, kv_width_b:], HEAD_B
    )
    attn_a = finish(state_a, query_a.shape[1])
    attn_b = finish(state_b, query_b.shape[1])
    own_rows = tok_rows // lax.axis_size("tp")
    own_start = lax.axis_index("tp") * own_rows
    head_sum = lax.psum(
        (
            jnp.dot(attn_a, out_a, preferred_element_type=jnp.float32)
            + jnp.dot(attn_b, out_b, preferred_element_type=jnp.float32)
        ).astype(jnp.bfloat16),
        "tp",
    ).astype(jnp.float32)
    whole_mixed = residual.astype(jnp.float32) + head_sum
    normed = normalize(whole_mixed, norm_gain)
    mixed_rows = lax.dynamic_slice_in_dim(whole_mixed, own_start, own_rows, 0)
    pieces = (
        lax.all_gather(gate_weight, "sp", axis=0, tiled=True),
        lax.all_gather(up_weight, "sp", axis=0, tiled=True),
    )
    gate_act = jnp.dot(normed, pieces[0], preferred_element_type=jnp.float32)
    up_act = jnp.dot(normed, pieces[1], preferred_element_type=jnp.float32)
    hidden = (jax.nn.silu(gate_act) * up_act).astype(jnp.bfloat16)
    down_all = jnp.dot(
        hidden,
        lax.all_gather(down_weight, "sp", axis=1, tiled=True),
        preferred_element_type=jnp.float32,
    )
    branch_sum = lax.psum_scatter(
        down_all.astype(jnp.bfloat16), "tp", scatter_dimension=0, tiled=True
    ).astype(jnp.float32)
    return (mixed_rows + 0.5 * branch_sum).astype(jnp.bfloat16)


def solution(mesh):
    return jax.shard_map(
        on_device,
        mesh=mesh,
        in_specs=(
            P("sp", "tp"),
            P("sp", "tp"),
            P("sp", "tp"),
            P("sp", "tp"),
            P("sp", "tp"),
            P("sp", "tp"),
            P(),
            P(),
            P("tp", None),
            P("tp", None),
            P("sp", None),
            P(),
            P("sp", "tp"),
            P("sp", "tp"),
            P("tp", "sp"),
        ),
        out_specs=P(("sp", "tp"), None),
        check_vma=False,
    )
```

profile of v0, /device:TPU:0, one launch (start us, length us, event | category | flops | bytes accessed | tf_op | source)
XLA Modules:
  0.0 724.6 jit_solution(1680261890716808169)
XLA Ops:
  7.4 1.0 copy.39
  8.4 0.8 slice_reduce_fusion
  9.5 0.9 copy.40
  10.9 33.9 %all_gather.20 = bf16[1536,256]{1,0:T(8,128)(2,1)S(1)} all-gather(bf16[192,256]{1,0:T(8,128)(2,1)S(1)} %copy.41), channel_id=1, replica_groups=mesh['sp'=8,'tp'=4] {'sp'}, dimensions={0}, use_global_device_ids=true | all-gather | bytes 884736 | tf_op jit(solution)/shard_map/all_gather | solution.py:114
  45.8 5.1 bitcast_reduce_fusion
  52.1 0.2 fusion.46
  52.6 32.3 %all_gather.18 = bf16[1536,256]{1,0:T(8,128)(2,1)S(1)} all-gather(bf16[192,256]{1,0:T(8,128)(2,1)S(1)} %copy.31), channel_id=1, replica_groups=mesh['sp'=8,'tp'=4] {'sp'}, dimensions={0}, use_global_device_ids=true | all-gather | bytes 884736 | tf_op jit(solution)/shard_map/all_gather | solution.py:112
  84.9 0.3 copy.32
  85.5 3.1 bitcast_reduce_fusion.1
  88.5 32.2 %all_gather.19 = bf16[1536,256]{1,0:T(8,128)(2,1)S(1)} all-gather(bf16[192,256]{1,0:T(8,128)(2,1)S(1)} %copy-done.6), channel_id=1, replica_groups=mesh['sp'=8,'tp'=4] {'sp'}, dimensions={0}, use_global_device_ids=true | all-gather | bytes 884736 | tf_op jit(solution)/shard_map/all_gather | solution.py:113
  120.7 0.3 copy.36
  121.0 3.4 fusion.7
  124.4 0.3 copy-done
  124.8 1.0 fusion.23
  126.1 5.4 fusion.1
  131.5 5.7 fusion.29
  137.2 1.0 fusion.57
  138.2 1.2 copy-done.2
  139.4 2.2 fusion.3
  141.7 0.5 all-gather.4.cloned.1.call-update
  142.2 0.5 all-gather.6.cloned.1.call-update
  142.8 0.5 all-gather.8.cloned.1.call-update
  143.4 0.3 reduce-scatter.2.cloned.1.call-start
  143.6 41.4 %all-reduce.2.cloned.1.call-done = bf16[192,4096]{1,0:T(8,128)(2,1)} async-done(((bf16[192,4096]{1,0:T(8,128)(2,1)}), bf16[192,4096]{1,0:T(8,128)(2,1)}) %all-reduce.2.cloned.1.call-update) | async-done | bytes 1572880 | tf_op jit(solution)/shard_map/psum | solution.py:124
  185.1 2.5 convert_add_fusion
  187.6 133.1 %all-gather.4.cloned.1.call-done = bf16[4096,1536]{1,0:T(8,128)(2,1)} async-done(((bf16[512,1536]{1,0:T(8,128)(2,1)}), bf16[4096,1536]{1,0:T(8,128)(2,1)}) %all-gather.4.cloned.1.call-update) | async-done | bytes 12582928 | tf_op jit(solution)/shard_map/all_gather | solution.py:135
  320.7 9.2 %fusion.55 = f32[192,1536]{1,0:T(8,128)} fusion(bf16[4096,1536]{1,0:T(8,128)(2,1)} %all-gather.4.cloned.1.call-done, f32[4096]{0:T(1024)S(1)} %copy-done.8, f32[192]{0:T(256)S(1)} %add_rsqrt_fusion.4, bf16[192,4096]{1,0:T(8,128)(2,1)} %all-reduce.2.cloned.1.call-done, bf16[192,4096]{1,0:T(8,128)(2,1)} %param.25), kind=kOutput, calls=%fused_computation.121 | convolution fusion | flops 2420637696 | bytes 16925440 | tf_op jit(solution)/shard_map/dot_general | solution.py:138
  329.9 167.0 %all-gather.6.cloned.1.call-done = bf16[4096,1536]{1,0:T(8,128)(2,1)} async-done(((bf16[512,1536]{1,0:T(8,128)(2,1)}), bf16[4096,1536]{1,0:T(8,128)(2,1)}) %all-gather.6.cloned.1.call-update) | async-done | bytes 12582928 | tf_op jit(solution)/shard_map/all_gather | solution.py:136
  496.9 176.0 %all-gather.8.cloned.1.call-done = bf16[1536,4096]{1,0:T(8,128)(2,1)} async-done(((bf16[1536,512]{1,0:T(8,128)(2,1)}), bf16[1536,4096]{1,0:T(8,128)(2,1)}) %all-gather.8.cloned.1.call-update) | async-done | bytes 12582928 | tf_op jit(solution)/shard_map/all_gather | solution.py:143
  672.9 15.9 %convolution_convert_fusion = bf16[192,4096]{1,0:T(8,128)(2,1)} fusion(bf16[1536,4096]{1,0:T(8,128)(2,1)} %all-gather.8.cloned.1.call-done, bf16[4096,1536]{1,0:T(8,128)(2,1)} %all-gather.6.cloned.1.call-done, f32[192,1536]{1,0:T(8,128)} %fusion.55, f32[4096]{0:T(1024)S(1)} %copy-done.8, f32[192]{0:T(256)S(1)} %add_rsqrt_fusion.4, ...), kind=kOutput, calls=%fused_computation.7 | convolution fusion | flops 4839112704 | bytes 31081216 | tf_op jit(solution)/shard_map/dot_general | solution.py:141
  688.8 26.4 %reduce-scatter.2.cloned.1.call-done = bf16[48,4096]{1,0:T(8,128)(2,1)} async-done(((bf16[192,4096]{1,0:T(8,128)(2,1)}), bf16[48,4096]{1,0:T(8,128)(2,1)}) %reduce-scatter.2.cloned.1.call-update) | async-done | bytes 393232 | tf_op jit(solution)/shard_map/reduce_scatter | solution.py:146
  715.2 1.8 add_convert_fusion
  (77 shorter events, 3.8 us)
Async XLA Ops:
  7.4 37.6 %copy-start.3 = (bf16[192,512]{1,0:T(8,128)(2,1)S(1)}, bf16[192,512]{1,0:T(8,128)(2,1)}, u32[]{:S(2)}) copy-start(bf16[192,512]{1,0:T(8,128)(2,1)} %param.18) | copy-start | bytes 589828
  7.4 177.7 %all-reduce.2.cloned.1.call-start = ((), (), s32[]{:S(2)}) async-start(), calls=%async_computation.1 | async-start | bytes 3145728 | tf_op jit(solution)/shard_map/psum | solution.py:124
  45.8 5.3 copy-start.4
  45.8 5.5 copy-start.7
  50.9 0.9 copy-start.5
  85.4 3.1 copy-start.6
  121.0 3.8 copy-start
  131.4 5.7 copy-start.1
  137.2 2.2 copy-start.2
  141.6 179.1 %all-gather.4.cloned.1.call-start = ((), (), s32[]{:S(2)}) async-start(), calls=%async_computation.2 | async-start | bytes 14155776 | tf_op jit(solution)/shard_map/all_gather | solution.py:135
  142.2 354.7 %all-gather.6.cloned.1.call-start = ((), (), s32[]{:S(2)}) async-start(), calls=%async_computation.3 | async-start | bytes 14155776 | tf_op jit(solution)/shard_map/all_gather | solution.py:136
  142.8 530.2 %all-gather.8.cloned.1.call-start = ((), (), s32[]{:S(2)}) async-start(), calls=%async_computation.4 | async-start | bytes 14155776 | tf_op jit(solution)/shard_map/all_gather | solution.py:143
  143.4 177.3 %copy-start.8 = (f32[4096]{0:T(1024)S(1)}, f32[4096]{0:T(1024)}, u32[]{:S(2)}) copy-start(f32[4096]{0:T(1024)} %param.26) | copy-start | bytes 49156
  143.4 571.8 %reduce-scatter.2.cloned.1.call-start = ((), (), s32[]{:S(2)}) async-start(), calls=%async_computation.5 | async-start | bytes 1966080 | tf_op jit(solution)/shard_map/reduce_scatter | solution.py:146
Sparse Core Ops, SparseCore 0:
  141.7 43.2 all-reduce.1
  688.9 26.2 reduce-scatter.1
Sparse Core Ops, SparseCore 1:
  144.3 176.3 all-gather.3
  322.8 174.1 all-gather.5
  498.8 174.1 all-gather.7
where the time goes:
time: 725 us
  waiting for transfers between devices  546 us (75%)
  blocking collectives  98.4 us (14%)
  matrix products  43.1 us (6%)
  between operations  15.4 us (2%)
  other arithmetic  15.1 us (2%)
    all_gather x1, waiting for transfers between devices, on_device(): lax.all_gather(down_weight, 'sp', axis=1, tiled=True)  176 us
    all_gather x1, waiting for transfers between devices, on_device(): lax.all_gather(up_weight, 'sp', axis=0, tiled=True)  167 us
    all_gather x1, waiting for transfers between devices, on_device(): lax.all_gather(gate_weight, 'sp', axis=0, tiled=True)  133 us
    psum x1, waiting for transfers between devices, on_device(): lax.psum((jnp.dot(attn_a, out_a, preferred_element_type=jnp.float32) + jn...  41.4 us
    all_gather x1, blocking collectives, on_device(): lax.all_gather(pair_b, 'sp', axis=0, tiled=True)  33.9 us
    all_gather x1, blocking collectives, on_device(): lax.all_gather(turned_ka, 'sp', axis=0, tiled=True)  32.3 us
    all_gather x1, blocking collectives, on_device(): lax.all_gather(value_a, 'sp', axis=0, tiled=True)  32.2 us
    reduce_scatter x1, waiting for transfers between devices, on_device(): lax.psum_scatter(down_all.astype(jnp.bfloat16), 'tp', scatter_dimension=0...  26.4 us
  transfers between devices with their start and end apart: 5, of which 5 were waited for; matrix products, arithmetic and copies ran while one was open for 2% of the time, Pallas kernels for 0%

commit v1 on v0

--- a/solution.py
+++ b/solution.py
@@ -103,49 +103,60 @@
     turned_ka = rotate(key_a, kv_heads_a, HEAD_A, first_pos, gain_a[1])
     turned_qb = rotate(query_b, heads_b, HEAD_B, first_pos, gain_b[0])
     turned_kb = rotate(key_b, kv_heads_b, HEAD_B, first_pos, gain_b[1])
-    pair_b = jnp.concatenate([turned_kb, value_b], axis=1)
+    widths = (key_a.shape[1], value_a.shape[1], key_b.shape[1], value_b.shape[1])
+    cuts = [sum(widths[:i]) for i in range(5)]
+    sp = lax.axis_size("sp")
+    tp = lax.axis_size("tp")
+    ff_own = gate_weight.shape[1] // sp
+    both = jnp.concatenate(
+        [
+            gate_weight.reshape(gate_weight.shape[0], sp, ff_own),
+            up_weight.reshape(up_weight.shape[0], sp, ff_own),
+        ],
+        axis=2,
+    ).transpose(1, 0, 2)
+    both = lax.all_to_all(both, "sp", 0, 0, tiled=True).reshape(-1, 2 * ff_own)
+    pairs = lax.all_gather(
+        jnp.concatenate([turned_ka, value_a, turned_kb, value_b], axis=1), "sp", axis=0, tiled=True
+    )
     initial = (
         start_state(kv_heads_a, heads_a // kv_heads_a, tok_rows, HEAD_A),
         start_state(kv_heads_b, heads_b // kv_heads_b, tok_rows, HEAD_B),
     )
-    pieces = (
-        lax.all_gather(turned_ka, "sp", axis=0, tiled=True),
-        lax.all_gather(value_a, "sp", axis=0, tiled=True),
-        lax.all_gather(pair_b, "sp", axis=0, tiled=True),
-    )
+    pieces = [pairs[:, cuts[i] : cuts[i + 1]] for i in range(4)]
     state_a = attend(initial[0], turned_qa, pieces[0], pieces[1], HEAD_A)
-    state_b = attend(
-        initial[1], turned_qb, pieces[2][:, :kv_width_b], pieces[2][:, kv_width_b:], HEAD_B
-    )
+    state_b = attend(initial[1], turned_qb, pieces[2], pieces[3], HEAD_B)
     attn_a = finish(state_a, query_a.shape[1])
     attn_b = finish(state_b, query_b.shape[1])
-    own_rows = tok_rows // lax.axis_size("tp")
+    own_rows = tok_rows // tp
     own_start = lax.axis_index("tp") * own_rows
-    head_sum = lax.psum(
+    head_sum = lax.psum_scatter(
         (
             jnp.dot(attn_a, out_a, preferred_element_type=jnp.float32)
             + jnp.dot(attn_b, out_b, preferred_element_type=jnp.float32)
         ).astype(jnp.bfloat16),
         "tp",
+        scatter_dimension=0,
+        tiled=True,
     ).astype(jnp.float32)
-    whole_mixed = residual.astype(jnp.float32) + head_sum
-    normed = normalize(whole_mixed, norm_gain)
-    mixed_rows = lax.dynamic_slice_in_dim(whole_mixed, own_start, own_rows, 0)
-    pieces = (
-        lax.all_gather(gate_weight, "sp", axis=0, tiled=True),
-        lax.all_gather(up_weight, "sp", axis=0, tiled=True),
+    mixed_rows = (
+        lax.dynamic_slice_in_dim(residual, own_start, own_rows, 0).astype(jnp.float32) + head_sum
     )
-    gate_act = jnp.dot(normed, pieces[0], preferred_element_type=jnp.float32)
-    up_act = jnp.dot(normed, pieces[1], preferred_element_type=jnp.float32)
-    hidden = (jax.nn.silu(gate_act) * up_act).astype(jnp.bfloat16)
-    down_all = jnp.dot(
-        hidden,
-        lax.all_gather(down_weight, "sp", axis=1, tiled=True),
-        preferred_element_type=jnp.float32,
-    )
-    branch_sum = lax.psum_scatter(
-        down_all.astype(jnp.bfloat16), "tp", scatter_dimension=0, tiled=True
-    ).astype(jnp.float32)
+    normed = lax.all_gather(normalize(mixed_rows, norm_gain), ("sp", "tp"), axis=0, tiled=True)
+    acts = jnp.dot(normed, both, preferred_element_type=jnp.float32)
+    hidden = (jax.nn.silu(acts[:, :ff_own]) * acts[:, ff_own:]).astype(jnp.bfloat16)
+    hidden = lax.all_gather(hidden, "sp", axis=0)
+    down_rows = down_weight.reshape(sp, ff_own, down_weight.shape[1])
+    down_all = jnp.einsum("smk,skn->mn", hidden, down_rows, preferred_element_type=jnp.float32)
+    cols = down_weight.shape[1]
+    branch = lax.psum_scatter(
+        down_all.astype(jnp.bfloat16).reshape(sp, tp, own_rows, cols).transpose(1, 0, 2, 3),
+        "tp",
+        scatter_dimension=0,
+        tiled=True,
+    ).reshape(sp, own_rows, cols)
+    branch_sum = lax.all_to_all(branch, "sp", 0, 0, tiled=True).transpose(1, 0, 2)
+    branch_sum = branch_sum.reshape(own_rows, sp * cols).astype(jnp.float32)
     return (mixed_rows + 0.5 * branch_sum).astype(jnp.bfloat16)
 
 

time: 725 us -> 416 us (0.57)
  waiting for transfers between devices: 546 us -> 183 us
  blocking collectives: 98.4 us -> 150 us
  local copies, waits for them, and re-layouts: 6.61 us -> 32.7 us
  matrix products: 43.1 us -> 21.7 us
    all_gather x3, waiting for transfers between devices: 476 us -> 130 us  [the longest x1 77.8 us: on_device(): hidden = lax.all_gather(hidden, 'sp', axis=0)]
    all_to_all x0 -> x2, blocking collectives: none -> 150 us  [the longest x1 132 us: on_device(): both = lax.all_to_all(both, 'sp', 0, 0, tiled=True).reshape(-1, 2 * ff_own)]
    all_gather x3 -> x0, blocking collectives: 98.4 us -> none  [the longest x1 33.9 us: on_device(): lax.all_gather(pair_b, 'sp', axis=0, tiled=True)]
    psum x1 -> x0, waiting for transfers between devices: 41.4 us -> none  [on_device(): lax.psum((jnp.dot(attn_a, out_a, preferred_element_type=jnp.float32) + jn...]
    reduce_scatter x1 -> x2, waiting for transfers between devices: 26.4 us -> 53.1 us  [the longest x1 26.6 us: on_device(): lax.psum_scatter((jnp.dot(attn_a, out_a, preferred_element_type=jnp.float...]
    dot_general x2, matrix products: 25.1 us -> 11.9 us  [the longest x1 9.03 us: on_device(): acts = jnp.dot(normed, both, preferred_element_type=jnp.float32)]
    unnamed x23 -> x35, local copies, waits for them, and re-layouts: 3.88 us -> 15.9 us
  transfers between devices with their start and end apart: 5 -> 5, of which waited for: 5 -> 4; matrix products, arithmetic and copies ran while one was open for 2% -> 3% of each run, Pallas kernels for 0% -> 0%
where the time goes in v1:
time: 416 us; the launch traced here: 415 us
  waiting for transfers between devices  183 us (44%)
  blocking collectives  150 us (36%)
  local copies, waits for them, and re-layouts  32.7 us (8%)
  matrix products  21.7 us (5%)
  other arithmetic  14 us (3%)
  between operations  13.6 us (3%)
    all_to_all x1, blocking collectives, on_device(): both = lax.all_to_all(both, 'sp', 0, 0, tiled=True).reshape(-1, 2 * ff_own)  132 us
    all_gather x1, waiting for transfers between devices, on_device(): hidden = lax.all_gather(hidden, 'sp', axis=0)  77.8 us
    all_gather x1, waiting for transfers between devices, on_device(): lax.all_gather(jnp.concatenate([turned_ka, value_a, turned_kb, value_b],...  51.7 us
    reduce_scatter x1, waiting for transfers between devices, on_device(): lax.psum_scatter((jnp.dot(attn_a, out_a, preferred_element_type=jnp.float...  26.6 us
    reduce_scatter x1, waiting for transfers between devices, on_device(): lax.psum_scatter(down_all.astype(jnp.bfloat16).reshape(sp, tp, own_rows,...  26.5 us
    all_to_all x1, blocking collectives, on_device(): lax.all_to_all(branch, 'sp', 0, 0, tiled=True).transpose(1, 0, 2)  17.4 us
    unnamed x35, local copies, waits for them, and re-layouts  15.9 us
    dot_general x1, matrix products, on_device(): acts = jnp.dot(normed, both, preferred_element_type=jnp.float32)  9.03 us
  transfers between devices with their start and end apart: 5, of which 4 were waited for; matrix products, arithmetic and copies ran while one was open for 3% of the time, Pallas kernels for 0%

profile of v1, /device:TPU:0, one launch (start us, length us, event | category | flops | bytes accessed | tf_op | source)
XLA Modules:
  0.0 414.6 jit_solution(11499507578292080837)
XLA Ops:
  10.6 1.0 copy.37
  11.6 1.0 copy.39
  17.4 51.7 %all-gather.5.cloned.1.call-done = bf16[1536,768]{1,0:T(8,128)(2,1)} async-done(((bf16[192,768]{1,0:T(8,128)(2,1)}), bf16[1536,768]{1,0:T(8,128)(2,1)}) %all-gather.5.cloned.1.call-update) | async-done | bytes 2359312 | tf_op jit(solution)/shard_map/all_gather | solution.py:119
  69.1 2.4 fusion.56
  71.5 1.4 copy.67
  72.9 2.1 fusion.55
  74.9 1.2 copy.49
  76.1 1.9 copy.51
  78.0 1.2 copy.68
  79.2 1.9 bitcast_reduce_fusion.1
  83.4 1.6 bitcast_reduce_fusion
  85.5 1.0 fusion.57
  86.5 1.7 fusion.1
  88.3 2.1 fusion.31
  90.5 2.2 fusion.3
  92.7 26.6 %reduce-scatter.3.cloned.1.call-done = bf16[48,4096]{1,0:T(8,128)(2,1)} async-done(((bf16[192,4096]{1,0:T(8,128)(2,1)}), bf16[48,4096]{1,0:T(8,128)(2,1)}) %reduce-scatter.3.cloned.1.call-update) | async-done | bytes 393232 | tf_op jit(solution)/shard_map/reduce_scatter | solution.py:133
  119.3 1.2 multiply_reduce_fusion
  120.6 1.9 multiply_convert_fusion
  122.7 1.7 copy.52
  124.5 2.6 copy.53
  127.1 1.6 maximum_bitcast_fusion
  128.7 132.1 %all_to_all.10 = bf16[8,512,384]{1,2,0:T(8,128)(2,1)} all-to-all(bf16[8,512,384]{1,2,0:T(8,128)(2,1)S(1)} %maximum_bitcast_fusion), channel_id=1, replica_groups=mesh['sp'=8,'tp'=4] {'sp'}, dimensions={0} | all-to-all | bytes 6291456 | tf_op jit(solution)/shard_map/all_to_all | solution.py:118
  260.8 4.7 %copy.54 = bf16[8,512,384]{2,1,0:T(8,128)(2,1)} copy(bf16[8,512,384]{1,2,0:T(8,128)(2,1)} %all_to_all.10) | data formatting | bytes 6291456 | tf_op jit(solution)/shard_map/all_to_all | solution.py:118
  265.5 9.0 %fusion.58 = f32[1536,384]{0,1:T(8,128)S(1)} fusion(bf16[1536,4096]{1,0:T(8,128)(2,1)} %all-gather.7.cloned.1.call-done, bf16[4096,384]{1,0:T(8,128)(2,1)} %bitcast.214), kind=kOutput, calls=%fused_computation.127 | convolution fusion | flops 4831838208 | bytes 18087936 | tf_op jit(solution)/shard_map/dot_general | solution.py:146
  274.6 1.2 fusion.21
  275.8 77.8 %all-gather.9.cloned.1.call-done = bf16[12288,192]{0,1:T(8,128)(2,1)} async-done(((bf16[1536,192]{0,1:T(8,128)(2,1)}), bf16[12288,192]{0,1:T(8,128)(2,1)}) %all-gather.9.cloned.1.call-update) | async-done | bytes 4718608 | tf_op jit(solution)/shard_map/all_gather | solution.py:148
  353.7 4.2 %copy.70 = bf16[24,8,8,1536]{3,2,1,0:T(8,128)(2,1)S(1)} copy(bf16[24,8,8,1536]{3,1,2,0:T(8,128)(2,1)} %bitcast.209) | data formatting | bytes 9437184
  357.9 2.9 fusion.9
  360.8 1.3 copy.74
  362.1 26.5 %reduce-scatter.5.cloned.1.call-done = bf16[1,8,48,512]{3,2,1,0:T(8,128)(2,1)} async-done(((bf16[4,8,48,512]{3,2,1,0:T(8,128)(2,1)}), bf16[1,8,48,512]{3,2,1,0:T(8,128)(2,1)}) %reduce-scatter.5.cloned.1.call-update) | async-done | bytes 393232 | tf_op jit(solution)/shard_map/reduce_scatter | solution.py:152
  388.6 17.4 %all_to_all.11 = bf16[8,48,512]{2,1,0:T(8,128)(2,1)S(1)} all-to-all(bf16[8,48,512]{2,1,0:T(8,128)(2,1)} %bitcast.224), channel_id=1, replica_groups=mesh['sp'=8,'tp'=4] {'sp'}, dimensions={0} | all-to-all | bytes 786432 | tf_op jit(solution)/shard_map/all_to_all | solution.py:158
  406.2 1.9 add_convert_fusion
  (93 shorter events, 12.0 us)
Async XLA Ops:
  6.5 351.4 %copy-start = (bf16[1536,512]{1,0:T(8,128)(2,1)S(1)}, bf16[1536,512]{1,0:T(8,128)(2,1)}, u32[]{:S(2)}) copy-start(bf16[1536,512]{1,0:T(8,128)(2,1)} %param.29) | copy-start | bytes 4718596
  6.5 8.1 %copy-start.9 = (bf16[192,512]{1,0:T(8,128)(2,1)S(1)}, bf16[192,512]{1,0:T(8,128)(2,1)}, u32[]{:S(2)}) copy-start(bf16[192,512]{1,0:T(8,128)(2,1)} %param.15) | copy-start | bytes 589828
  6.5 8.3 %copy-start.10 = (bf16[192,512]{1,0:T(8,128)(2,1)S(1)}, bf16[192,512]{1,0:T(8,128)(2,1)}, u32[]{:S(2)}) copy-start(bf16[192,512]{1,0:T(8,128)(2,1)} %param.18) | copy-start | bytes 589828
  6.5 62.5 %all-gather.5.cloned.1.call-start = ((), (), s32[]{:S(2)}) async-start(), calls=%async_computation.4 | async-start | bytes 2654208 | tf_op jit(solution)/shard_map/all_gather | solution.py:119
  14.4 105.0 %reduce-scatter.3.cloned.1.call-start = ((), (), s32[]{:S(2)}) async-start(), calls=%async_computation.5 | async-start | bytes 1966080 | tf_op jit(solution)/shard_map/reduce_scatter | solution.py:133
  79.2 2.9 copy-start.7
  82.0 1.3 copy-start.5
  83.4 2.2 copy-start.2
  86.5 1.7 copy-start.8
  88.3 2.2 copy-start.3
  90.5 28.9 %copy-start.6 = (bf16[192,4096]{1,0:T(8,128)(2,1)S(1)}, bf16[192,4096]{1,0:T(8,128)(2,1)}, u32[]{:S(2)}) copy-start(bf16[192,4096]{1,0:T(8,128)(2,1)} %param.25) | copy-start | bytes 4718596
  90.5 30.1 %copy-start.11 = (f32[4096]{0:T(1024)S(1)}, f32[4096]{0:T(1024)}, u32[]{:S(2)}) copy-start(f32[4096]{0:T(1024)} %param.26) | copy-start | bytes 49156
  92.7 172.9 %all-gather.7.cloned.1.call-start = ((), (), s32[]{:S(2)}) async-start(), calls=%async_computation.6 | async-start | bytes 12976128 | tf_op jit(solution)/shard_map/all_gather | solution.py:145
  122.5 231.2 %all-gather.9.cloned.1.call-start = ((), (), s32[]{:S(2)}) async-start(), calls=%async_computation.8 | async-start | bytes 5308416 | tf_op jit(solution)/shard_map/all_gather | solution.py:148
  275.8 112.8 %reduce-scatter.5.cloned.1.call-start = ((), (), s32[]{:S(2)}) async-start(), calls=%async_computation.7 | async-start | bytes 1966080 | tf_op jit(solution)/shard_map/reduce_scatter | solution.py:152
  360.8 45.4 %copy-start.4 = (bf16[48,4096]{1,0:T(8,128)(2,1)S(1)}, bf16[48,4096]{1,0:T(8,128)(2,1)}, u32[]{:S(2)}) copy-start(bf16[48,4096]{1,0:T(8,128)(2,1)} %reduce-scatter.3.cloned.1.call-done) | copy-start | bytes 1179652
  360.8 47.3 %copy-start.1 = (bf16[1536,512]{1,0:T(8,128)(2,1)S(1)}, bf16[1536,512]{1,0:T(8,128)(2,1)}, u32[]{:S(2)}) copy-start(bf16[1536,512]{1,0:T(8,128)(2,1)} %param.29) | copy-start | bytes 4718596
Sparse Core Ops, SparseCore 0:
  14.5 54.5 all-gather.4
  92.8 26.4 reduce-scatter.2
  122.6 141.2 all-gather.6
  275.9 77.7 all-gather.8
  362.2 26.3 reduce-scatter.4

commit v2 on v1

--- a/solution.py
+++ b/solution.py
@@ -143,11 +143,16 @@
         lax.dynamic_slice_in_dim(residual, own_start, own_rows, 0).astype(jnp.float32) + head_sum
     )
     normed = lax.all_gather(normalize(mixed_rows, norm_gain), ("sp", "tp"), axis=0, tiled=True)
-    acts = jnp.dot(normed, both, preferred_element_type=jnp.float32)
-    hidden = (jax.nn.silu(acts[:, :ff_own]) * acts[:, ff_own:]).astype(jnp.bfloat16)
-    hidden = lax.all_gather(hidden, "sp", axis=0)
-    down_rows = down_weight.reshape(sp, ff_own, down_weight.shape[1])
-    down_all = jnp.einsum("smk,skn->mn", hidden, down_rows, preferred_element_type=jnp.float32)
+    acts = lax.dot_general(
+        both, normed, (((0,), (1,)), ((), ())), preferred_element_type=jnp.float32
+    )
+    hidden = (jax.nn.silu(acts[:ff_own]) * acts[ff_own:]).astype(jnp.bfloat16)
+    down_all = lax.dot_general(
+        lax.all_gather(hidden, "sp", axis=0, tiled=True),
+        down_weight,
+        (((0,), (0,)), ((), ())),
+        preferred_element_type=jnp.float32,
+    )
     cols = down_weight.shape[1]
     branch = lax.psum_scatter(
         down_all.astype(jnp.bfloat16).reshape(sp, tp, own_rows, cols).transpose(1, 0, 2, 3),

time: 416 us -> 414 us (level)
  local copies, waits for them, and re-layouts: 32.7 us -> 28.5 us
    unnamed x35 -> x32, local copies, waits for them, and re-layouts: 15.9 us -> 11.6 us
where the time goes in v2:
time: 414 us; the launch traced here: 413 us
  waiting for transfers between devices  183 us (44%)
  blocking collectives  150 us (36%)
  local copies, waits for them, and re-layouts  28.5 us (7%)
  matrix products  23.8 us (6%)
  other arithmetic  14 us (3%)
  between operations  13.6 us (3%)
    all_to_all x1, blocking collectives, on_device(): both = lax.all_to_all(both, 'sp', 0, 0, tiled=True).reshape(-1, 2 * ff_own)  132 us
    all_gather x1, waiting for transfers between devices, on_device(): lax.all_gather(hidden, 'sp', axis=0, tiled=True)  77.8 us
    all_gather x1, waiting for transfers between devices, on_device(): lax.all_gather(jnp.concatenate([turned_ka, value_a, turned_kb, value_b],...  51.7 us
    reduce_scatter x1, waiting for transfers between devices, on_device(): lax.psum_scatter((jnp.dot(attn_a, out_a, preferred_element_type=jnp.float...  26.6 us
    reduce_scatter x1, waiting for transfers between devices, on_device(): lax.psum_scatter(down_all.astype(jnp.bfloat16).reshape(sp, tp, own_rows,...  26.6 us
    all_to_all x1, blocking collectives, on_device(): lax.all_to_all(branch, 'sp', 0, 0, tiled=True).transpose(1, 0, 2)  17.4 us
    unnamed x32, local copies, waits for them, and re-layouts  11.6 us
    dot_general x1, matrix products, on_device(): lax.dot_general(both, normed, (((0,), (1,)), ((), ())), preferred_element...  9.06 us
  transfers between devices with their start and end apart: 5, of which 4 were waited for; matrix products, arithmetic and copies ran while one was open for 3% of the time, Pallas kernels for 0%

profile of v2, /device:TPU:0, one launch (start us, length us, event | category | flops | bytes accessed | tf_op | source)
XLA Modules:
  0.0 412.6 jit_solution(15568090273182111965)
XLA Ops:
  10.6 1.0 copy.35
  11.6 1.0 copy.37
  17.4 51.7 %all-gather.4.cloned.1.call-done = bf16[1536,768]{1,0:T(8,128)(2,1)} async-done(((bf16[192,768]{1,0:T(8,128)(2,1)}), bf16[1536,768]{1,0:T(8,128)(2,1)}) %all-gather.4.cloned.1.call-update) | async-done | bytes 2359312 | tf_op jit(solution)/shard_map/all_gather | solution.py:119
  69.1 2.4 fusion.54
  71.5 1.4 copy.64
  72.9 2.1 fusion.53
  74.9 1.2 copy.47
  76.1 1.9 copy.49
  78.0 1.2 copy.65
  79.2 1.9 bitcast_reduce_fusion.1
  82.1 1.0 fusion.23
  83.4 1.6 bitcast_reduce_fusion
  85.5 1.0 fusion.55
  86.5 1.7 fusion.1
  88.3 2.1 fusion.29
  90.5 2.2 fusion.3
  92.7 26.6 %reduce-scatter.3.cloned.1.call-done = bf16[48,4096]{1,0:T(8,128)(2,1)} async-done(((bf16[192,4096]{1,0:T(8,128)(2,1)}), bf16[48,4096]{1,0:T(8,128)(2,1)}) %reduce-scatter.3.cloned.1.call-update) | async-done | bytes 393232 | tf_op jit(solution)/shard_map/reduce_scatter | solution.py:133
  119.3 1.2 multiply_reduce_fusion
  120.6 1.9 multiply_convert_fusion
  122.7 1.7 copy.50
  124.5 2.6 copy.51
  127.1 1.6 maximum_bitcast_fusion
  128.7 132.1 %all_to_all.10 = bf16[8,512,384]{1,2,0:T(8,128)(2,1)} all-to-all(bf16[8,512,384]{1,2,0:T(8,128)(2,1)S(1)} %maximum_bitcast_fusion), channel_id=1, replica_groups=mesh['sp'=8,'tp'=4] {'sp'}, dimensions={0} | all-to-all | bytes 6291456 | tf_op jit(solution)/shard_map/all_to_all | solution.py:118
  260.8 4.7 %copy.52 = bf16[8,512,384]{2,1,0:T(8,128)(2,1)} copy(bf16[8,512,384]{1,2,0:T(8,128)(2,1)} %all_to_all.10) | data formatting | bytes 6291456 | tf_op jit(solution)/shard_map/all_to_all | solution.py:118
  265.5 9.1 %fusion.56 = f32[384,1536]{1,0:T(8,128)S(1)} fusion(bf16[4096,384]{1,0:T(8,128)(2,1)} %bitcast.203, bf16[1536,4096]{1,0:T(8,128)(2,1)} %all-gather.6.cloned.1.call-done), kind=kOutput, calls=%fused_computation.125 | convolution fusion | flops 4831838208 | bytes 18087936 | tf_op jit(solution)/shard_map/dot_general | solution.py:146
  274.6 1.2 fusion.19
  275.9 77.8 %all-gather.8.cloned.1.call-done = bf16[1536,1536]{1,0:T(8,128)(2,1)} async-done(((bf16[192,1536]{1,0:T(8,128)(2,1)}), bf16[1536,1536]{1,0:T(8,128)(2,1)}) %all-gather.8.cloned.1.call-update) | async-done | bytes 4718608 | tf_op jit(solution)/shard_map/all_gather | solution.py:151
  353.7 5.0 %convolution_convert_fusion = bf16[1536,512]{1,0:T(8,128)(2,1)S(1)} fusion(bf16[1536,1536]{1,0:T(8,128)(2,1)} %all-gather.8.cloned.1.call-done, bf16[1536,512]{1,0:T(8,128)(2,1)S(1)} %copy-done), kind=kOutput, calls=%fused_computation.14 | convolution fusion | flops 2416705536 | bytes 7864320 | tf_op jit(solution)/shard_map/dot_general | solution.py:150
  358.7 1.3 copy.68
  360.0 26.6 %reduce-scatter.5.cloned.1.call-done = bf16[1,8,48,512]{3,2,1,0:T(8,128)(2,1)} async-done(((bf16[4,8,48,512]{3,2,1,0:T(8,128)(2,1)}), bf16[1,8,48,512]{3,2,1,0:T(8,128)(2,1)}) %reduce-scatter.5.cloned.1.call-update) | async-done | bytes 393232 | tf_op jit(solution)/shard_map/reduce_scatter | solution.py:157
  386.6 17.4 %all_to_all.11 = bf16[8,48,512]{2,1,0:T(8,128)(2,1)S(1)} all-to-all(bf16[8,48,512]{2,1,0:T(8,128)(2,1)} %bitcast.213), channel_id=1, replica_groups=mesh['sp'=8,'tp'=4] {'sp'}, dimensions={0} | all-to-all | bytes 786432 | tf_op jit(solution)/shard_map/all_to_all | solution.py:163
  404.2 1.9 add_convert_fusion
  (90 shorter events, 11.0 us)
Async XLA Ops:
  6.5 347.1 %copy-start = (bf16[1536,512]{1,0:T(8,128)(2,1)S(1)}, bf16[1536,512]{1,0:T(8,128)(2,1)}, u32[]{:S(2)}) copy-start(bf16[1536,512]{1,0:T(8,128)(2,1)} %param.29) | copy-start | bytes 4718596
  6.5 8.1 %copy-start.8 = (bf16[192,512]{1,0:T(8,128)(2,1)S(1)}, bf16[192,512]{1,0:T(8,128)(2,1)}, u32[]{:S(2)}) copy-start(bf16[192,512]{1,0:T(8,128)(2,1)} %param.15) | copy-start | bytes 589828
  6.5 8.3 %copy-start.9 = (bf16[192,512]{1,0:T(8,128)(2,1)S(1)}, bf16[192,512]{1,0:T(8,128)(2,1)}, u32[]{:S(2)}) copy-start(bf16[192,512]{1,0:T(8,128)(2,1)} %param.18) | copy-start | bytes 589828
  6.5 62.5 %all-gather.4.cloned.1.call-start = ((), (), s32[]{:S(2)}) async-start(), calls=%async_computation.4 | async-start | bytes 2654208 | tf_op jit(solution)/shard_map/all_gather | solution.py:119
  14.4 105.0 %reduce-scatter.3.cloned.1.call-start = ((), (), s32[]{:S(2)}) async-start(), calls=%async_computation.5 | async-start | bytes 1966080 | tf_op jit(solution)/shard_map/reduce_scatter | solution.py:133
  79.2 2.9 copy-start.6
  82.0 1.3 copy-start.4
  83.4 2.2 copy-start.1
  86.5 1.7 copy-start.7
  88.3 2.2 copy-start.2
  90.5 28.9 %copy-start.5 = (bf16[192,4096]{1,0:T(8,128)(2,1)S(1)}, bf16[192,4096]{1,0:T(8,128)(2,1)}, u32[]{:S(2)}) copy-start(bf16[192,4096]{1,0:T(8,128)(2,1)} %param.25) | copy-start | bytes 4718596
  90.5 30.1 %copy-start.10 = (f32[4096]{0:T(1024)S(1)}, f32[4096]{0:T(1024)}, u32[]{:S(2)}) copy-start(f32[4096]{0:T(1024)} %param.26) | copy-start | bytes 49156
  92.7 172.9 %all-gather.6.cloned.1.call-start = ((), (), s32[]{:S(2)}) async-start(), calls=%async_computation.6 | async-start | bytes 12976128 | tf_op jit(solution)/shard_map/all_gather | solution.py:145
  122.5 231.2 %all-gather.8.cloned.1.call-start = ((), (), s32[]{:S(2)}) async-start(), calls=%async_computation.7 | async-start | bytes 5308416 | tf_op jit(solution)/shard_map/all_gather | solution.py:151
  275.8 110.8 %reduce-scatter.5.cloned.1.call-start = ((), (), s32[]{:S(2)}) async-start(), calls=%async_computation.8 | async-start | bytes 1966080 | tf_op jit(solution)/shard_map/reduce_scatter | solution.py:157
  358.7 45.5 %copy-start.3 = (bf16[48,4096]{1,0:T(8,128)(2,1)S(1)}, bf16[48,4096]{1,0:T(8,128)(2,1)}, u32[]{:S(2)}) copy-start(bf16[48,4096]{1,0:T(8,128)(2,1)} %reduce-scatter.3.cloned.1.call-done) | copy-start | bytes 1179652
Sparse Core Ops, SparseCore 0:
  14.5 54.5 all-gather.3
  92.8 26.4 reduce-scatter.2
  122.6 141.2 all-gather.5
  275.9 77.6 all-gather.7
  360.1 26.4 reduce-scatter.4
